TPU v7x, 512 devices: a whole 4x8x8 slice. The times are simulated.
512 devices in a mesh: ep: 128 (over z, y, core), tp: 4 (over x).
Axes of the slice: x: 4, y: 8, z: 8, core: 2. Of those that a mesh axis runs over, the one named last changes fastest.
Arguments:
- tokens: bfloat16 [256, 2048], P('ep'), may hold values from -6 to 6
- state_c: float32 [256, 8, 128, 256], P('ep', 'tp'), may hold values from -0.8 to 0.8
- state_n: float32 [256, 8, 128], P('ep', 'tp'), may hold values from -0.8 to 0.8
- state_m: float32 [256, 8], P('ep', 'tp'), may hold values from -2 to 2
- mix_gain: float32 [2048], replicated, may hold values from 0.1 to 1.9
- w_query: bfloat16 [2048, 1024], P('ep', 'tp'), may hold values from -0.125 to 0.125
- w_key: bfloat16 [2048, 1024], P('ep', 'tp'), may hold values from -0.125 to 0.125
- w_value: bfloat16 [2048, 2048], P('ep', 'tp'), may hold values from -0.125 to 0.125
- w_input_gate: bfloat16 [2048, 8], replicated, may hold values from -0.125 to 0.125
- w_forget_gate: bfloat16 [2048, 8], replicated, may hold values from -0.125 to 0.125
- forget_bias: float32 [8], replicated, may hold values from -1 to 4
- w_output: bfloat16 [2048, 2048], P('tp', 'ep'), may hold values from -0.125 to 0.125
- moe_gain: float32 [2048], replicated, may hold values from 0.1 to 1.9
- w_group: bfloat16 [2048, 4], replicated, may hold values from -0.25 to 0.25
- expert_ids: int32 [256, 2], P('ep'), may hold values from 0 to 127, all different within a row; in each aligned block of 2 rows (0 to 1, 2 to 3, ...) at most 1 rows name the same one
- expert_weight: float32 [256, 2], P('ep'), may hold values from 0.1 to 1
- w_exp_gate: bfloat16 [128, 2048, 512], P('ep', None, 'tp'), may hold values from -0.125 to 0.125
- w_exp_up: bfloat16 [128, 2048, 512], P('ep', None, 'tp'), may hold values from -0.25 to 0.25
- w_exp_down: bfloat16 [128, 512, 2048], P('ep', 'tp'), may hold values from -1 to 1
- w_dense: bfloat16 [2048, 2048], P('ep', 'tp'), may hold values from -0.125 to 0.125
- w_dense_gate: bfloat16 [2048], replicated, may hold values from -0.125 to 0.125
Outputs:
- mixed: bfloat16 [256, 2048], P('ep', 'tp')
- new_c: float32 [256, 8, 128, 256], P('ep', 'tp')
- new_n: float32 [256, 8, 128], P('ep', 'tp')
- new_m: float32 [256, 8], P('ep', 'tp')
Inputs may be any that keep to these rules, and one draw needn't show every extreme that they name: `expert_ids`: each row names 2 different experts. In each aligned block of 2 rows (the rows of one index of ep) no expert is named by more than 1 row, a bound that some block reaches. Every expert is named by some row.
All inputs are finite; a program needn't handle non-finite values.
Results may differ from a plain program's by a relative error of at most 0.025.
Values may be sent and summed in bfloat16 or wider, within the bound.
A program may use at most 64 MiB of HBM per device.

v0:
```python
import jax
import jax.numpy as jnp
from jax import lax
from jax.sharding import PartitionSpec as P

CAP = 1
eps = 1e-06


def side_by_side(arrays, axis, dim, along):
    both = jnp.concatenate(arrays, axis=along)
    filled, at, finished = (lax.all_gather(both, axis, axis=dim, tiled=True), 0, [])
    for a in arrays:
        finished.append(lax.slice_in_dim(filled, at, at + a.shape[along], axis=along))
        at += a.shape[along]
    return tuple(finished)


def copy_for_each(shard, axis):
    copies = jnp.broadcast_to(shard, (lax.axis_size(axis), *shard.shape))
    return lax.all_to_all(copies, axis, split_axis=0, concat_axis=0, tiled=True)


def over_copies(shard, axis):
    everything = copy_for_each(shard, axis)
    return jnp.sum(everything.astype(jnp.float32), axis=0)


def in_blocks(shard, dim, count):
    before, after = (shard.shape[:dim], shard.shape[dim + 1 :])
    return jnp.moveaxis(shard.reshape(*before, count, -1, *after), dim, 0)


def sum_at_owner(shard, axis, dim):
    tiles = in_blocks(shard, dim, lax.axis_size(axis))
    arrived = lax.all_to_all(tiles, axis, split_axis=0, concat_axis=0, tiled=True)
    return arrived.astype(jnp.float32).sum(axis=0)


def rms_norm(values, gain):
    widened = values.astype(jnp.float32)
    inverse = lax.rsqrt(jnp.mean(widened * widened, axis=-1, keepdims=True) + eps)
    return (widened * inverse * gain).astype(jnp.bfloat16)


def rounded(values):
    return lax.optimization_barrier(values.astype(jnp.bfloat16)).astype(jnp.float32)


def memory_step(query_rows, key_rows, value_rows, in_gate, forget, state_c, state_n, state_m):
    seq_count, head_count = state_m.shape
    q_heads = query_rows.reshape(seq_count, head_count, -1)
    k_heads = key_rows.reshape(seq_count, head_count, -1) * q_heads.shape[-1] ** (-0.5)
    v_heads = value_rows.reshape(seq_count, head_count, -1)
    new_m = jnp.maximum(forget + state_m, in_gate)
    decay = jnp.exp(forget + state_m - new_m)
    inflow = jnp.exp(in_gate - new_m)
    new_c = (
        decay[..., None, None] * state_c
        + (inflow[..., None] * k_heads)[..., :, None] * v_heads[..., None, :]
    )
    new_n = decay[..., None] * state_n + inflow[..., None] * k_heads
    numer = jnp.einsum("shd,shde->she", q_heads, new_c, precision=lax.Precision.HIGHEST)
    denom = jnp.maximum(jnp.abs(jnp.sum(q_heads * new_n, axis=-1)), 1.0)
    heads = (numer / denom[..., None]).astype(jnp.bfloat16).reshape(seq_count, -1)
    return (heads, new_c, new_n, new_m)


def per_device(
    tokens,
    state_c,
    state_n,
    state_m,
    mix_gain,
    w_query,
    w_key,
    w_value,
    w_input_gate,
    w_forget_gate,
    forget_bias,
    w_output,
    moe_gain,
    w_group,
    expert_ids,
    expert_weight,
    w_exp_gate,
    w_exp_up,
    w_exp_down,
    w_dense,
    w_dense_gate,
):
    seq_count = tokens.shape[0]
    width = tokens.shape[1]
    tp_count = lax.axis_size("tp")
    ep_count = lax.axis_size("ep")
    tp_rank = lax.axis_index("tp")
    head_count = state_m.shape[1]
    share = width // tp_count
    normed = rms_norm(tokens, mix_gain)
    pieces = side_by_side((w_query, w_key, w_value), "ep", 0, 1)
    feature_cols = normed
    query_sum, key_sum, value_sum = tuple(
        (
            jnp.dot(feature_cols, weight_rows, preferred_element_type=jnp.float32)
            for weight_rows in pieces
        )
    )
    query_rows = rounded(query_sum)
    key_rows = rounded(key_sum)
    value_rows = rounded(value_sum)
    gate_all = jnp.dot(normed, w_input_gate, preferred_element_type=jnp.float32)
    forget_all = jax.nn.log_sigmoid(
        jnp.dot(normed, w_forget_gate, preferred_element_type=jnp.float32) + forget_bias
    )
    in_gate = lax.dynamic_slice_in_dim(gate_all, tp_rank * head_count, head_count, 1)
    forget = lax.dynamic_slice_in_dim(forget_all, tp_rank * head_count, head_count, 1)
    heads, new_c, new_n, new_m = memory_step(
        query_rows, key_rows, value_rows, in_gate, forget, state_c, state_n, state_m
    )
    partial_value = jnp.dot(
        heads,
        lax.all_gather(w_output, "ep", axis=1, tiled=True),
        preferred_element_type=jnp.float32,
    )
    mixer_sum = over_copies(partial_value.astype(jnp.bfloat16), "tp").astype(jnp.float32)
    residual = (tokens.astype(jnp.float32) + mixer_sum).astype(jnp.bfloat16)
    normed2 = rms_norm(residual, moe_gain)
    group_count = w_group.shape[1]
    group_prob = jax.nn.softmax(
        jnp.dot(normed2, w_group, preferred_element_type=jnp.float32), axis=-1
    )
    experts_here = w_exp_gate.shape[0]
    expert_count = experts_here * ep_count
    per_group = expert_count // group_count
    top_count = expert_ids.shape[1]
    member = (expert_ids // per_group)[..., None] == jnp.arange(group_count, dtype=jnp.int32)[
        None, None, :
    ]
    picked = jnp.sum(jnp.where(member, group_prob[:, None, :], 0.0), axis=-1)
    route = picked * expert_weight / jnp.sum(expert_weight, axis=1, keepdims=True)
    flat_ids = expert_ids.reshape(-1)
    assigned = flat_ids[:, None] == jnp.arange(expert_count, dtype=jnp.int32)[None, :]
    ranks = jnp.cumsum(assigned.astype(jnp.int32), axis=0) - 1
    own_rank = jnp.sum(jnp.where(assigned, ranks, 0), axis=1)
    slot_index = flat_ids * CAP + own_rank
    placing = (
        jnp.arange(expert_count * CAP, dtype=jnp.int32)[:, None] == slot_index[None, :]
    ).astype(jnp.bfloat16)
    repeated = jnp.repeat(normed2, top_count, axis=0)
    outgoing = jnp.dot(placing, repeated, preferred_element_type=jnp.float32).astype(jnp.bfloat16)
    outgoing = outgoing.reshape(expert_count, CAP, width)
    arrived = lax.all_to_all(outgoing, "ep", split_axis=0, concat_axis=0, tiled=True)
    slots = arrived.shape[1]
    grid_rows = arrived.reshape(ep_count, experts_here, slots, width)
    gate_act = jnp.einsum(
        "sxnd,xdf->sxnf", grid_rows, w_exp_gate, preferred_element_type=jnp.float32
    )
    up_act = jnp.einsum("sxnd,xdf->sxnf", grid_rows, w_exp_up, preferred_element_type=jnp.float32)
    hidden = (jax.nn.silu(gate_act) * up_act).astype(jnp.bfloat16)
    down_part = jnp.einsum("sxnf,xfd->sxnd", hidden, w_exp_down, preferred_element_type=jnp.float32)
    reduced = sum_at_owner(down_part.astype(jnp.bfloat16), "tp", 3).astype(jnp.bfloat16)
    returned = lax.all_to_all(
        reduced.reshape(expert_count, slots, share), "ep", split_axis=0, concat_axis=0, tiled=True
    )
    picked_rows = jnp.einsum(
        "ca,cd->ad",
        placing,
        returned.reshape(expert_count * CAP, share),
        preferred_element_type=jnp.float32,
    )
    moe = jnp.sum(route[..., None] * picked_rows.reshape(seq_count, top_count, share), axis=1)
    feature_cols = normed2
    dense_raw = jnp.dot(
        feature_cols,
        lax.all_gather(w_dense, "ep", axis=0, tiled=True),
        preferred_element_type=jnp.float32,
    )
    dense_gate = jax.nn.sigmoid(jnp.dot(normed2, w_dense_gate, preferred_element_type=jnp.float32))
    own_cols = lax.dynamic_slice_in_dim(residual, tp_rank * share, share, 1).astype(jnp.float32)
    mixed = (own_cols + moe + dense_gate[:, None] * dense_raw).astype(jnp.bfloat16)
    return (mixed, new_c, new_n, new_m)


def solution(mesh):
    placed = (
        P("ep", None),
        P("ep", "tp", None, None),
        P("ep", "tp", None),
        P("ep", "tp"),
        P(),
        P("ep", "tp"),
        P("ep", "tp"),
        P("ep", "tp"),
        P(),
        P(),
        P(),
        P("tp", "ep"),
        P(),
        P(),
        P("ep", None),
        P("ep", None),
        P("ep", None, "tp"),
        P("ep", None, "tp"),
        P("ep", "tp", None),
        P("ep", "tp"),
        P(),
    )
    return jax.shard_map(
        per_device,
        mesh=mesh,
        in_specs=placed,
        out_specs=(P("ep", "tp"), P("ep", "tp", None, None), P("ep", "tp", None), P("ep", "tp")),
        check_vma=False,
    )
```

profile of v0, /device:TPU:1, one launch (start us, length us, event | category | flops | bytes accessed | tf_op | source)
XLA Modules:
  0.0 283.7 jit_solution(10336514559572382456)
XLA Ops:
  7.2 1.4 pad_maximum_fusion
  8.7 0.7 all-gather.6.cloned.1.call-update
  9.4 0.7 all-gather.8.cloned.1.call-update
  10.1 0.8 fusion.41
  11.0 0.8 fusion.43
  11.8 0.9 fusion.57
  12.7 0.9 fusion.49
  13.6 0.8 subtract_exponential_fusion.1
  14.4 0.8 reshape.144
  15.3 86.7 %all-gather.4.cloned.1.call-done = bf16[2048,1024]{1,0:T(8,128)(2,1)} async-done(((bf16[16,1024]{1,0:T(8,128)(2,1)}), bf16[2048,1024]{1,0:T(8,128)(2,1)}) %all-gather.4.cloned.1.call-update) | async-done | bytes 4194320 | tf_op jit(solution)/shard_map/all_gather | solution.py:12
  102.0 1.5 convolution_convert_fusion.4
  103.5 1.5 convolution_convert_fusion.3
  105.0 2.0 fusion.9
  107.1 0.7 multiply_reduce_fusion
  108.3 76.8 %all-gather.6.cloned.1.call-done = bf16[512,2048]{0,1:T(8,128)(2,1)} async-done(((bf16[512,16]{0,1:T(8,128)(2,1)}), bf16[512,2048]{0,1:T(8,128)(2,1)}) %all-gather.6.cloned.1.call-update) | async-done | bytes 2097168 | tf_op jit(solution)/shard_map/all_gather | solution.py:122
  185.1 2.2 convolution_convert_fusion.2
  188.0 4.0 %all-to-all-start = ((bf16[4,2,2048]{2,1,0:T(2,128)(2,1)}), bf16[4,2,2048]{2,1,0:T(2,128)(2,1)S(1)}, u32[]{:S(2)}, u32[]{:S(2)}) async-start(bf16[4,2,2048]{2,1,0:T(2,128)(2,1)} %broadcast_in_dim.15), calls=%async_computation | async-start | bytes 65536 | tf_op jit(solution)/shard_map/all_to_all | solution.py:21
  192.1 4.1 %all-to-all-done = bf16[4,2,2048]{2,1,0:T(2,128)(2,1)S(1)} async-done(((bf16[4,2,2048]{2,1,0:T(2,128)(2,1)}), bf16[4,2,2048]{2,1,0:T(2,128)(2,1)S(1)}, u32[]{:S(2)}, u32[]{:S(2)}) %all-to-all-start) | async-done | bytes 32800 | tf_op jit(solution)/shard_map/all_to_all | solution.py:21
  197.4 1.0 reduce.2
  198.4 1.2 reshape.167
  199.5 11.0 %all-to-all-start.1 = ((bf16[128,2,1024]{2,1,0:T(2,128)(2,1)}), bf16[128,2,1024]{2,1,0:T(2,128)(2,1)S(1)}, u32[]{:S(2)}, u32[]{:S(2)}) async-start(bf16[128,2,1024]{2,1,0:T(2,128)(2,1)} %reshape.167), calls=%async_computation.1 | async-start | bytes 1048576 | tf_op jit(solution)/shard_map/all_to_all | solution.py:152
  211.0 20.3 %all-to-all-done.1 = bf16[128,2,1024]{2,1,0:T(2,128)(2,1)S(1)} async-done(((bf16[128,2,1024]{2,1,0:T(2,128)(2,1)}), bf16[128,2,1024]{2,1,0:T(2,128)(2,1)S(1)}, u32[]{:S(2)}, u32[]{:S(2)}) %all-to-all-start.1) | async-done | bytes 524320 | tf_op jit(solution)/shard_map/all_to_all | solution.py:152
  232.2 0.7 convolution_convert_fusion
  232.9 0.8 copy.67
  233.7 3.5 %all-to-all-start.2 = ((bf16[4,128,1,1,512]{4,1,3,2,0:T(8,128)(2,1)}), bf16[4,128,1,1,512]{4,1,3,2,0:T(8,128)(2,1)S(1)}, u32[]{:S(2)}, u32[]{:S(2)}) async-start(bf16[4,128,1,1,512]{4,1,3,2,0:T(8,128)(2,1)} %bitcast.95), calls=%async_computation.2 | async-start | bytes 1048576 | tf_op jit(solution)/shard_map/all_to_all | solution.py:36
  237.6 9.3 %all-to-all-done.2 = bf16[4,128,1,1,512]{4,1,3,2,0:T(8,128)(2,1)S(1)} async-done(((bf16[4,128,1,1,512]{4,1,3,2,0:T(8,128)(2,1)}), bf16[4,128,1,1,512]{4,1,3,2,0:T(8,128)(2,1)S(1)}, u32[]{:S(2)}, u32[]{:S(2)}) %all-to-all-start.2) | async-done | bytes 524320 | tf_op jit(solution)/shard_map/all_to_all | solution.py:36
  247.0 0.7 reduce.3
  247.7 0.7 reshape.169
  248.4 5.8 %all-to-all-start.3 = ((bf16[128,2,256]{2,1,0:T(2,128)(2,1)}), bf16[128,2,256]{2,1,0:T(2,128)(2,1)S(1)}, u32[]{:S(2)}, u32[]{:S(2)}) async-start(bf16[128,2,256]{2,1,0:T(2,128)(2,1)} %reshape.169), calls=%async_computation.3 | async-start | bytes 262144 | tf_op jit(solution)/shard_map/all_to_all | solution.py:162
  254.4 13.1 %all-to-all-done.3 = bf16[128,2,256]{2,1,0:T(2,128)(2,1)S(1)} async-done(((bf16[128,2,256]{2,1,0:T(2,128)(2,1)}), bf16[128,2,256]{2,1,0:T(2,128)(2,1)S(1)}, u32[]{:S(2)}, u32[]{:S(2)}) %all-to-all-start.3) | async-done | bytes 131104 | tf_op jit(solution)/shard_map/all_to_all | solution.py:162
  267.8 6.8 %all-gather.8.cloned.1.call-done = bf16[2048,512]{1,0:T(8,128)(2,1)} async-done(((bf16[16,512]{1,0:T(8,128)(2,1)}), bf16[2048,512]{1,0:T(8,128)(2,1)}) %all-gather.8.cloned.1.call-update) | async-done | bytes 2097168 | tf_op jit(solution)/shard_map/all_gather | solution.py:175
  274.6 2.6 fusion.8
  (70 shorter events, 5.2 us)
Async XLA Ops:
  7.2 225.0 %copy-start = (bf16[1,128,2048]{2,1,0:T(8,128)(2,1)S(1)}, bf16[1,128,2048]{2,1,0:T(8,128)(2,1)}, u32[]{:S(2)}) copy-start(bf16[1,128,2048]{2,1,0:T(8,128)(2,1)} %param.39) | copy-start | bytes 1572868
  7.2 94.9 %all-gather.4.cloned.1.call-start = ((), (), s32[]{:S(2)}) async-start(), calls=%async_computation.4 | async-start | bytes 4227072 | tf_op jit(solution)/shard_map/all_gather | solution.py:12
  8.6 176.4 %all-gather.6.cloned.1.call-start = ((), (), s32[]{:S(2)}) async-start(), calls=%async_computation.5 | async-start | bytes 2113536 | tf_op jit(solution)/shard_map/all_gather | solution.py:122
  9.4 265.2 %all-gather.8.cloned.1.call-start = ((), (), s32[]{:S(2)}) async-start(), calls=%async_computation.6 | async-start | bytes 2113536 | tf_op jit(solution)/shard_map/all_gather | solution.py:175
  14.3 92.7 %copy-start.9 = (f32[2,2]{1,0:T(2,128)}, f32[2,2]{1,0:T(2,128)S(1)}, u32[]{:S(2)}) copy-start(f32[2,2]{1,0:T(2,128)S(1)} %get-tuple-element.10) | copy-start | bytes 52
  15.3 91.8 %copy-start.10 = (f32[2,2,128]{2,1,0:T(2,128)S(1)}, f32[2,2,128]{2,1,0:T(2,128)}, u32[]{:S(2)}) copy-start(f32[2,2,128]{2,1,0:T(2,128)} %param.23) | copy-start | bytes 6148
  15.3 92.4 %copy-start.2 = (f32[2,2,128,256]{3,2,1,0:T(8,128)S(1)}, f32[2,2,128,256]{3,2,1,0:T(8,128)}, u32[]{:S(2)}) copy-start(f32[2,2,128,256]{3,2,1,0:T(8,128)} %param.22) | copy-start | bytes 1572868
  107.0 89.3 %copy-start.5 = (bf16[2,2048]{1,0:T(2,128)(2,1)S(1)}, bf16[2,2048]{1,0:T(2,128)(2,1)}, u32[]{:S(2)}) copy-start(bf16[2,2048]{1,0:T(2,128)(2,1)} %param.21) | copy-start | bytes 24580
  107.0 89.4 %copy-start.6 = (f32[2048]{0:T(1024)S(1)}, f32[2048]{0:T(1024)}, u32[]{:S(2)}) copy-start(f32[2048]{0:T(1024)} %param.33) | copy-start | bytes 24580
  107.9 90.5 %copy-start.1 = (f32[2,2,128,256]{3,2,1,0:T(8,128)}, f32[2,2,128,256]{3,2,1,0:T(8,128)S(1)}, u32[]{:S(2)}) copy-start(f32[2,2,128,256]{3,2,1,0:T(8,128)S(1)} %multiply_add_fusion) | copy-start | bytes 1572868
  187.3 23.3 %copy-start.7 = (bf16[2048]{0:T(1024)(128)(2,1)S(1)}, bf16[2048]{0:T(1024)(128)(2,1)}, u32[]{:S(2)}) copy-start(bf16[2048]{0:T(1024)(128)(2,1)} %param.41) | copy-start | bytes 12292
  187.3 23.3 %copy-start.8 = (f32[2,2]{1,0:T(2,128)S(1)}, f32[2,2]{1,0:T(2,128)}, u32[]{:S(2)}) copy-start(f32[2,2]{1,0:T(2,128)} %param.36) | copy-start | bytes 52
  187.3 23.5 %copy-start.11 = (s32[2,2]{1,0:T(2,128)S(1)}, s32[2,2]{1,0:T(2,128)}, u32[]{:S(2)}) copy-start(s32[2,2]{1,0:T(2,128)} %param.35) | copy-start | bytes 52
  187.3 23.5 %copy-start.12 = (bf16[2048,4]{0,1:T(4,128)(2,1)S(1)}, bf16[2048,4]{0,1:T(4,128)(2,1)}, u32[]{:S(2)}) copy-start(bf16[2048,4]{0,1:T(4,128)(2,1)} %param.34) | copy-start | bytes 49156
  188.0 8.3 %all-to-all-start = ((bf16[4,2,2048]{2,1,0:T(2,128)(2,1)}), bf16[4,2,2048]{2,1,0:T(2,128)(2,1)S(1)}, u32[]{:S(2)}, u32[]{:S(2)}) async-start(bf16[4,2,2048]{2,1,0:T(2,128)(2,1)} %broadcast_in_dim.15), calls=%async_computation | async-start | bytes 65536 | tf_op jit(solution)/shard_map/all_to_all | solution.py:21
  198.4 33.4 %copy-start.3 = (bf16[1,2048,128]{2,1,0:T(8,128)(2,1)S(1)}, bf16[1,2048,128]{2,1,0:T(8,128)(2,1)}, u32[]{:S(2)}) copy-start(bf16[1,2048,128]{2,1,0:T(8,128)(2,1)} %param.37) | copy-start | bytes 1572868
  199.5 32.6 %copy-start.4 = (bf16[1,2048,128]{2,1,0:T(8,128)(2,1)S(1)}, bf16[1,2048,128]{2,1,0:T(8,128)(2,1)}, u32[]{:S(2)}) copy-start(bf16[1,2048,128]{2,1,0:T(8,128)(2,1)} %param.38) | copy-start | bytes 1572868
  199.5 31.7 %all-to-all-start.1 = ((bf16[128,2,1024]{2,1,0:T(2,128)(2,1)}), bf16[128,2,1024]{2,1,0:T(2,128)(2,1)S(1)}, u32[]{:S(2)}, u32[]{:S(2)}) async-start(bf16[128,2,1024]{2,1,0:T(2,128)(2,1)} %reshape.167), calls=%async_computation.1 | async-start | bytes 1048576 | tf_op jit(solution)/shard_map/all_to_all | solution.py:152
  233.7 13.2 %all-to-all-start.2 = ((bf16[4,128,1,1,512]{4,1,3,2,0:T(8,128)(2,1)}), bf16[4,128,1,1,512]{4,1,3,2,0:T(8,128)(2,1)S(1)}, u32[]{:S(2)}, u32[]{:S(2)}) async-start(bf16[4,128,1,1,512]{4,1,3,2,0:T(8,128)(2,1)} %bitcast.95), calls=%async_computation.2 | async-start | bytes 1048576 | tf_op jit(solution)/shard_map/all_to_all | solution.py:36
  248.4 19.1 %all-to-all-start.3 = ((bf16[128,2,256]{2,1,0:T(2,128)(2,1)}), bf16[128,2,256]{2,1,0:T(2,128)(2,1)S(1)}, u32[]{:S(2)}, u32[]{:S(2)}) async-start(bf16[128,2,256]{2,1,0:T(2,128)(2,1)} %reshape.169), calls=%async_computation.3 | async-start | bytes 262144 | tf_op jit(solution)/shard_map/all_to_all | solution.py:162
Sparse Core Ops, SparseCore 0:
  11.7 90.3 all-gather.3
  105.2 79.8 all-gather.5
  188.2 86.3 all-gather.7
where the time goes:
time: 285 us; the launch traced here: 284 us
  waiting for transfers between devices  219 us (77%)
  starting transfers between devices  24.3 us (9%)
  between operations  14 us (5%)
  matrix products  13.7 us (5%)
  other arithmetic  7.77 us (3%)
  local copies, waits for them, and re-layouts  5.32 us (2%)
    all_gather x1, waiting for transfers between devices, side_by_side(): lax.all_gather(both, axis, axis=dim, tiled=True)  86.7 us
    all_gather x1, waiting for transfers between devices, per_device(): lax.all_gather(w_output, 'ep', axis=1, tiled=True)  76.8 us
    all_to_all x1, waiting for transfers between devices, per_device(): lax.all_to_all(outgoing, 'ep', split_axis=0, concat_axis=0, tiled=True)  20.3 us
    all_to_all x1, waiting for transfers between devices, per_device(): lax.all_to_all(reduced.reshape(expert_count, slots, share), 'ep', split_a...  13.1 us
    all_to_all x1, starting transfers between devices, per_device(): lax.all_to_all(outgoing, 'ep', split_axis=0, concat_axis=0, tiled=True)  11 us
    all_to_all x1, waiting for transfers between devices, sum_at_owner(): lax.all_to_all(tiles, axis, split_axis=0, concat_axis=0, tiled=True)  9.33 us
    all_gather x1, waiting for transfers between devices, per_device(): lax.all_gather(w_dense, 'ep', axis=0, tiled=True)  6.85 us
    all_to_all x1, starting transfers between devices, per_device(): lax.all_to_all(reduced.reshape(expert_count, slots, share), 'ep', split_a...  5.81 us
  transfers between devices with their start and end apart: 7, of which 7 were waited for; matrix products, arithmetic and copies ran while one was open for 8% of the time, Pallas kernels for 0%

commit v1 on v0

--- a/solution.py
+++ b/solution.py
@@ -5,6 +5,12 @@
 
 CAP = 1
 eps = 1e-06
+connect_slices = lambda local_values, bus_axis, where_dim: jnp.concatenate(
+    lax.all_to_all(
+        jnp.stack([local_values for _ in range(lax.axis_size(bus_axis))]), bus_axis, 0, 0
+    ),
+    axis=where_dim,
+)
 
 
 def side_by_side(arrays, axis, dim, along):
@@ -118,9 +124,7 @@
         query_rows, key_rows, value_rows, in_gate, forget, state_c, state_n, state_m
     )
     partial_value = jnp.dot(
-        heads,
-        lax.all_gather(w_output, "ep", axis=1, tiled=True),
-        preferred_element_type=jnp.float32,
+        heads, connect_slices(w_output, "ep", 1), preferred_element_type=jnp.float32
     )
     mixer_sum = over_copies(partial_value.astype(jnp.bfloat16), "tp").astype(jnp.float32)
     residual = (tokens.astype(jnp.float32) + mixer_sum).astype(jnp.bfloat16)

time: 285 us -> 231 us (0.81)
  waiting for transfers between devices: 219 us -> 149 us
  starting transfers between devices: 24.3 us -> 42.8 us
  matrix products: 13.7 us -> 10.6 us
    all_gather x1 -> x0, waiting for transfers between devices: 76.8 us -> none  [per_device(): lax.all_gather(w_output, 'ep', axis=1, tiled=True)]
    all_to_all x0 -> x1, starting transfers between devices: none -> 18.6 us  [lax.all_to_all(jnp.stack([local_values for _ in range(lax.axis_size(bus_a...]
    all_gather x1, waiting for transfers between devices: 86.7 us -> 99.6 us  [side_by_side(): lax.all_gather(both, axis, axis=dim, tiled=True)]
    all_gather x1, waiting for transfers between devices: 6.85 us -> 2.01 us  [per_device(): lax.all_gather(w_dense, 'ep', axis=0, tiled=True)]
  transfers between devices with their start and end apart: 7 -> 7, of which waited for: 7 -> 6; matrix products, arithmetic and copies ran while one was open for 8% -> 9% of each run, Pallas kernels for 0% -> 0%
where the time goes in v1:
time: 231 us; the launch traced here: 230 us
  waiting for transfers between devices  149 us (65%)
  starting transfers between devices  42.8 us (19%)
  between operations  14.3 us (6%)
  matrix products  10.6 us (5%)
  local copies, waits for them, and re-layouts  6.97 us (3%)
  other arithmetic  6.71 us (3%)
    all_gather x1, waiting for transfers between devices, side_by_side(): lax.all_gather(both, axis, axis=dim, tiled=True)  99.6 us
    all_to_all x1, waiting for transfers between devices, per_device(): lax.all_to_all(outgoing, 'ep', split_axis=0, concat_axis=0, tiled=True)  20.1 us
    all_to_all x1, starting transfers between devices, lax.all_to_all(jnp.stack([local_values for _ in range(lax.axis_size(bus_a...  18.6 us
    all_to_all x1, waiting for transfers between devices, per_device(): lax.all_to_all(reduced.reshape(expert_count, slots, share), 'ep', split_a...  13 us
    all_to_all x1, starting transfers between devices, per_device(): lax.all_to_all(outgoing, 'ep', split_axis=0, concat_axis=0, tiled=True)  10.9 us
    all_to_all x1, waiting for transfers between devices, sum_at_owner(): lax.all_to_all(tiles, axis, split_axis=0, concat_axis=0, tiled=True)  9.32 us
    all_to_all x1, starting transfers between devices, per_device(): lax.all_to_all(reduced.reshape(expert_count, slots, share), 'ep', split_a...  5.82 us
    dot_general x3, matrix products, per_device(): jnp.dot(feature_cols, weight_rows, preferred_element_type=jnp.float32)  4.91 us
  transfers between devices with their start and end apart: 7, of which 6 were waited for; matrix products, arithmetic and copies ran while one was open for 9% of the time, Pallas kernels for 0%

profile of v1, /device:TPU:1, one launch (start us, length us, event | category | flops | bytes accessed | tf_op | source)
XLA Modules:
  0.0 230.3 jit_solution(421292995663037281)
XLA Ops:
  7.2 1.4 pad_maximum_fusion
  8.6 2.3 %stack.2 = bf16[128,512,16]{1,2,0:T(8,128)(2,1)} broadcast(bf16[512,16]{0,1:T(8,128)(2,1)} %param.32), dimensions={1,2} | broadcast | bytes 2113536 | tf_op jit(solution)/shard_map/stack | solution.py:10
  11.0 18.6 %all-to-all-start = ((bf16[128,512,16]{1,2,0:T(8,128)(2,1)}), bf16[128,512,16]{1,2,0:T(8,128)(2,1)S(1)}, u32[]{:S(2)}, u32[]{:S(2)}) async-start(bf16[128,512,16]{1,2,0:T(8,128)(2,1)} %stack.2), calls=%async_computation | async-start | bytes 4194304 | tf_op jit(solution)/shard_map/all_to_all | solution.py:9
  29.6 0.7 all-gather.5.cloned.1.call-update
  31.2 99.6 %all-gather.3.cloned.1.call-done = bf16[2048,1024]{1,0:T(8,128)(2,1)} async-done(((bf16[16,1024]{1,0:T(8,128)(2,1)}), bf16[2048,1024]{1,0:T(8,128)(2,1)}) %all-gather.3.cloned.1.call-update) | async-done | bytes 4194320 | tf_op jit(solution)/shard_map/all_gather | solution.py:18
  130.8 1.5 convolution_convert_fusion.4
  132.3 1.5 convolution_convert_fusion.3
  133.8 2.0 fusion.9
  135.8 0.7 multiply_reduce_fusion
  136.5 1.2 multiply_add_fusion
  137.7 0.3 fusion.58
  138.1 0.6 convolution_convert_fusion.2
  138.8 0.6 broadcast_in_dim.15
  139.4 4.0 %all-to-all-start.1 = ((bf16[4,2,2048]{2,1,0:T(2,128)(2,1)}), bf16[4,2,2048]{2,1,0:T(2,128)(2,1)S(1)}, u32[]{:S(2)}, u32[]{:S(2)}) async-start(bf16[4,2,2048]{2,1,0:T(2,128)(2,1)} %broadcast_in_dim.15), calls=%async_computation.1 | async-start | bytes 65536 | tf_op jit(solution)/shard_map/all_to_all | solution.py:27
  143.5 4.1 %all-to-all-done.1 = bf16[4,2,2048]{2,1,0:T(2,128)(2,1)S(1)} async-done(((bf16[4,2,2048]{2,1,0:T(2,128)(2,1)}), bf16[4,2,2048]{2,1,0:T(2,128)(2,1)S(1)}, u32[]{:S(2)}, u32[]{:S(2)}) %all-to-all-start.1) | async-done | bytes 32800 | tf_op jit(solution)/shard_map/all_to_all | solution.py:27
  148.2 0.5 broadcast.109
  148.8 1.0 reduce.2
  149.8 1.2 reshape.177
  150.9 10.9 %all-to-all-start.2 = ((bf16[128,2,1024]{2,1,0:T(2,128)(2,1)}), bf16[128,2,1024]{2,1,0:T(2,128)(2,1)S(1)}, u32[]{:S(2)}, u32[]{:S(2)}) async-start(bf16[128,2,1024]{2,1,0:T(2,128)(2,1)} %reshape.177), calls=%async_computation.2 | async-start | bytes 1048576 | tf_op jit(solution)/shard_map/all_to_all | solution.py:156
  162.4 20.1 %all-to-all-done.2 = bf16[128,2,1024]{2,1,0:T(2,128)(2,1)S(1)} async-done(((bf16[128,2,1024]{2,1,0:T(2,128)(2,1)}), bf16[128,2,1024]{2,1,0:T(2,128)(2,1)S(1)}, u32[]{:S(2)}, u32[]{:S(2)}) %all-to-all-start.2) | async-done | bytes 524320 | tf_op jit(solution)/shard_map/all_to_all | solution.py:156
  182.5 0.4 reshape.178
  183.0 0.4 convolution_bitcast_fusion.1
  183.4 0.7 convolution_convert_fusion
  184.1 0.8 copy.68
  184.9 3.5 %all-to-all-start.3 = ((bf16[4,128,1,1,512]{4,1,3,2,0:T(8,128)(2,1)}), bf16[4,128,1,1,512]{4,1,3,2,0:T(8,128)(2,1)S(1)}, u32[]{:S(2)}, u32[]{:S(2)}) async-start(bf16[4,128,1,1,512]{4,1,3,2,0:T(8,128)(2,1)} %bitcast.98), calls=%async_computation.3 | async-start | bytes 1048576 | tf_op jit(solution)/shard_map/all_to_all | solution.py:42
  188.8 9.3 %all-to-all-done.3 = bf16[4,128,1,1,512]{4,1,3,2,0:T(8,128)(2,1)S(1)} async-done(((bf16[4,128,1,1,512]{4,1,3,2,0:T(8,128)(2,1)}), bf16[4,128,1,1,512]{4,1,3,2,0:T(8,128)(2,1)S(1)}, u32[]{:S(2)}, u32[]{:S(2)}) %all-to-all-start.3) | async-done | bytes 524320 | tf_op jit(solution)/shard_map/all_to_all | solution.py:42
  198.2 0.7 reduce.3
  198.9 0.7 reshape.179
  199.6 5.8 %all-to-all-start.4 = ((bf16[128,2,256]{2,1,0:T(2,128)(2,1)}), bf16[128,2,256]{2,1,0:T(2,128)(2,1)S(1)}, u32[]{:S(2)}, u32[]{:S(2)}) async-start(bf16[128,2,256]{2,1,0:T(2,128)(2,1)} %reshape.179), calls=%async_computation.4 | async-start | bytes 262144 | tf_op jit(solution)/shard_map/all_to_all | solution.py:166
  205.6 13.0 %all-to-all-done.4 = bf16[128,2,256]{2,1,0:T(2,128)(2,1)S(1)} async-done(((bf16[128,2,256]{2,1,0:T(2,128)(2,1)}), bf16[128,2,256]{2,1,0:T(2,128)(2,1)S(1)}, u32[]{:S(2)}, u32[]{:S(2)}) %all-to-all-start.4) | async-done | bytes 131104 | tf_op jit(solution)/shard_map/all_to_all | solution.py:166
  218.9 2.0 all-gather.5.cloned.1.call-done
  220.9 2.6 %fusion.8 = bf16[2,512]{1,0:T(2,128)(2,1)} fusion(bf16[2,2048]{1,0:T(2,128)(2,1)S(1)} %fusion.40, bf16[2048,512]{1,0:T(8,128)(2,1)} %all-gather.5.cloned.1.call-done, f32[2,512]{1,0:T(2,128)S(1)} %fusion.6, f32[2]{0:T(128)S(1)} %fusion.16, bf16[2,2048]{1,0:T(2,128)(2,1)S(1)} %get-tuple-element.5, s32[]{:T(128)S(6)} %select_n.27), kind=kOutput, calls=%fused_computation.15 | convolution fusion | flops 4199424 | bytes 2113548 | tf_op jit(solution)/shard_map/dot_general | solution.py:177
  (78 shorter events, 3.4 us)
Async XLA Ops:
  7.2 176.2 %copy-start = (bf16[1,128,2048]{2,1,0:T(8,128)(2,1)S(1)}, bf16[1,128,2048]{2,1,0:T(8,128)(2,1)}, u32[]{:S(2)}) copy-start(bf16[1,128,2048]{2,1,0:T(8,128)(2,1)} %param.39) | copy-start | bytes 1572868
  7.2 123.7 %all-gather.3.cloned.1.call-start = ((), (), s32[]{:S(2)}) async-start(), calls=%async_computation.5 | async-start | bytes 4227072 | tf_op jit(solution)/shard_map/all_gather | solution.py:18
  11.0 19.4 %copy-start.11 = (s32[2,2]{1,0:T(2,128)S(1)}, s32[2,2]{1,0:T(2,128)}, u32[]{:S(2)}) copy-start(s32[2,2]{1,0:T(2,128)} %param.35) | copy-start | bytes 52
  11.0 19.6 %copy-start.4 = (bf16[2,2048]{1,0:T(2,128)(2,1)S(1)}, bf16[2,2048]{1,0:T(2,128)(2,1)}, u32[]{:S(2)}) copy-start(bf16[2,2048]{1,0:T(2,128)(2,1)} %param.21) | copy-start | bytes 24580
  11.0 19.7 %copy-start.5 = (f32[2048]{0:T(1024)S(1)}, f32[2048]{0:T(1024)}, u32[]{:S(2)}) copy-start(f32[2048]{0:T(1024)} %param.25) | copy-start | bytes 24580
  11.0 19.8 %copy-start.13 = (bf16[2048,8]{0,1:T(8,128)(2,1)S(1)}, bf16[2048,8]{0,1:T(8,128)(2,1)}, u32[]{:S(2)}) copy-start(bf16[2048,8]{0,1:T(8,128)(2,1)} %param.29) | copy-start | bytes 98308
  11.0 19.9 %copy-start.14 = (bf16[2048,8]{0,1:T(8,128)(2,1)S(1)}, bf16[2048,8]{0,1:T(8,128)(2,1)}, u32[]{:S(2)}) copy-start(bf16[2048,8]{0,1:T(8,128)(2,1)} %param.30) | copy-start | bytes 98308
  11.0 19.9 %copy-start.16 = (f32[8]{0:T(128)S(1)}, f32[8]{0:T(128)}, u32[]{:S(2)}) copy-start(f32[8]{0:T(128)} %param.31) | copy-start | bytes 100
  11.0 20.1 %copy-start.12 = (f32[2,2]{1,0:T(2,128)S(1)}, f32[2,2]{1,0:T(2,128)}, u32[]{:S(2)}) copy-start(f32[2,2]{1,0:T(2,128)} %param.24) | copy-start | bytes 52
  11.0 127.1 %all-to-all-start = ((bf16[128,512,16]{1,2,0:T(8,128)(2,1)}), bf16[128,512,16]{1,2,0:T(8,128)(2,1)S(1)}, u32[]{:S(2)}, u32[]{:S(2)}) async-start(bf16[128,512,16]{1,2,0:T(8,128)(2,1)} %stack.2), calls=%async_computation | async-start | bytes 4194304 | tf_op jit(solution)/shard_map/all_to_all | solution.py:9
  29.6 191.3 %all-gather.5.cloned.1.call-start = ((), (), s32[]{:S(2)}) async-start(), calls=%async_computation.6 | async-start | bytes 2113536 | tf_op jit(solution)/shard_map/all_gather | solution.py:179
  31.1 104.7 %copy-start.9 = (f32[2,2]{1,0:T(2,128)}, f32[2,2]{1,0:T(2,128)S(1)}, u32[]{:S(2)}) copy-start(f32[2,2]{1,0:T(2,128)S(1)} %get-tuple-element.10) | copy-start | bytes 52
  31.2 104.6 %copy-start.10 = (f32[2,2,128]{2,1,0:T(2,128)S(1)}, f32[2,2,128]{2,1,0:T(2,128)}, u32[]{:S(2)}) copy-start(f32[2,2,128]{2,1,0:T(2,128)} %param.23) | copy-start | bytes 6148
  135.8 12.0 %copy-start.6 = (f32[2048]{0:T(1024)S(1)}, f32[2048]{0:T(1024)}, u32[]{:S(2)}) copy-start(f32[2048]{0:T(1024)} %param.33) | copy-start | bytes 24580
  137.7 12.1 %copy-start.1 = (f32[2,2,128,256]{3,2,1,0:T(8,128)}, f32[2,2,128,256]{3,2,1,0:T(8,128)S(1)}, u32[]{:S(2)}) copy-start(f32[2,2,128,256]{3,2,1,0:T(8,128)S(1)} %multiply_add_fusion) | copy-start | bytes 1572868
  138.7 23.2 %copy-start.7 = (bf16[2048]{0:T(1024)(128)(2,1)S(1)}, bf16[2048]{0:T(1024)(128)(2,1)}, u32[]{:S(2)}) copy-start(bf16[2048]{0:T(1024)(128)(2,1)} %param.41) | copy-start | bytes 12292
  138.7 23.3 %copy-start.8 = (f32[2,2]{1,0:T(2,128)S(1)}, f32[2,2]{1,0:T(2,128)}, u32[]{:S(2)}) copy-start(f32[2,2]{1,0:T(2,128)} %param.36) | copy-start | bytes 52
  138.7 23.4 %copy-start.15 = (bf16[2048,4]{0,1:T(4,128)(2,1)S(1)}, bf16[2048,4]{0,1:T(4,128)(2,1)}, u32[]{:S(2)}) copy-start(bf16[2048,4]{0,1:T(4,128)(2,1)} %param.34) | copy-start | bytes 49156
  139.4 8.3 %all-to-all-start.1 = ((bf16[4,2,2048]{2,1,0:T(2,128)(2,1)}), bf16[4,2,2048]{2,1,0:T(2,128)(2,1)S(1)}, u32[]{:S(2)}, u32[]{:S(2)}) async-start(bf16[4,2,2048]{2,1,0:T(2,128)(2,1)} %broadcast_in_dim.15), calls=%async_computation.1 | async-start | bytes 65536 | tf_op jit(solution)/shard_map/all_to_all | solution.py:27
  149.8 33.2 %copy-start.2 = (bf16[1,2048,128]{2,1,0:T(8,128)(2,1)S(1)}, bf16[1,2048,128]{2,1,0:T(8,128)(2,1)}, u32[]{:S(2)}) copy-start(bf16[1,2048,128]{2,1,0:T(8,128)(2,1)} %param.37) | copy-start | bytes 1572868
  150.9 32.5 %copy-start.3 = (bf16[1,2048,128]{2,1,0:T(8,128)(2,1)S(1)}, bf16[1,2048,128]{2,1,0:T(8,128)(2,1)}, u32[]{:S(2)}) copy-start(bf16[1,2048,128]{2,1,0:T(8,128)(2,1)} %param.38) | copy-start | bytes 1572868
  150.9 31.6 %all-to-all-start.2 = ((bf16[128,2,1024]{2,1,0:T(2,128)(2,1)}), bf16[128,2,1024]{2,1,0:T(2,128)(2,1)S(1)}, u32[]{:S(2)}, u32[]{:S(2)}) async-start(bf16[128,2,1024]{2,1,0:T(2,128)(2,1)} %reshape.177), calls=%async_computation.2 | async-start | bytes 1048576 | tf_op jit(solution)/shard_map/all_to_all | solution.py:156
  184.9 13.2 %all-to-all-start.3 = ((bf16[4,128,1,1,512]{4,1,3,2,0:T(8,128)(2,1)}), bf16[4,128,1,1,512]{4,1,3,2,0:T(8,128)(2,1)S(1)}, u32[]{:S(2)}, u32[]{:S(2)}) async-start(bf16[4,128,1,1,512]{4,1,3,2,0:T(8,128)(2,1)} %bitcast.98), calls=%async_computation.3 | async-start | bytes 1048576 | tf_op jit(solution)/shard_map/all_to_all | solution.py:42
  199.6 19.0 %all-to-all-start.4 = ((bf16[128,2,256]{2,1,0:T(2,128)(2,1)}), bf16[128,2,256]{2,1,0:T(2,128)(2,1)S(1)}, u32[]{:S(2)}, u32[]{:S(2)}) async-start(bf16[128,2,256]{2,1,0:T(2,128)(2,1)} %reshape.179), calls=%async_computation.4 | async-start | bytes 262144 | tf_op jit(solution)/shard_map/all_to_all | solution.py:166
Sparse Core Ops, SparseCore 0:
  11.7 119.1 all-gather.2
  134.0 86.8 all-gather.4
